TPU v7x, 32 devices: a whole 2x2x4 slice. The times are simulated.
32 devices in a mesh: rep: 4 (over z), fs: 2 (over y), tp: 4 (over x, core).
Axes of the slice: x: 2, y: 2, z: 4, core: 2. Of those that a mesh axis runs over, the one named last changes fastest.
Arguments:
- inputs: bfloat16 [2560, 2048], P('rep', 'fs'), may hold values from -6 to 6
- gate_pre: bfloat16 [2560, 5632], P('rep', 'tp'), may hold values from -12 to 12
- up_pre: bfloat16 [2560, 5632], P('rep', 'tp'), may hold values from -6 to 6
- cotangent: bfloat16 [2560, 2048], P('rep'), may hold values from -6 to 6
- w_gate: bfloat16 [2048, 5632], P('fs', 'tp'), may hold values from -0.125 to 0.125
- w_up: bfloat16 [2048, 5632], P('fs', 'tp'), may hold values from -0.125 to 0.125
- w_down: bfloat16 [5632, 2048], P('tp', 'fs'), may hold values from -0.078125 to 0.078125
Outputs:
- grad_input: bfloat16 [2560, 2048], P('rep', 'fs')
- grad_gate: float32 [512, 4, 5632], P('fs', 'rep', 'tp')
- grad_up: float32 [512, 4, 5632], P('fs', 'rep', 'tp')
- grad_down: float32 [5632, 512, 4], P('tp', 'fs', 'rep')
- gate_norms: float32 [512, 4], P('fs', 'rep')
- up_norms: float32 [512, 4], P('fs', 'rep')
- down_norms: float32 [5632], P('tp')
All inputs are finite; a program needn't handle non-finite values.
Results may differ from a plain program's by a relative error of at most 0.02.
Values may be sent and summed in bfloat16 or wider, within the bound.
A program may use at most 64 MiB of HBM per device.

v0:
```python
import jax
import jax.numpy as jnp
from jax import lax
from jax.sharding import PartitionSpec as P


def on_device(inputs, gate_pre, up_pre, cotangent, w_gate, w_up, w_down):
    single = jnp.float32
    groups = lax.axis_size("rep")
    width = w_down.shape[1]
    own_cot = lax.dynamic_slice_in_dim(cotangent, lax.axis_index("fs") * width, width, 1)
    partial_grad = jnp.einsum("td,fd->tf", own_cot, w_down, preferred_element_type=single)
    hidden_grad = lax.psum(partial_grad.astype(jnp.bfloat16), "fs").astype(jnp.float32)
    gate = gate_pre.astype(single)
    upper = up_pre.astype(single)
    sigma = jax.nn.sigmoid(gate)
    active = gate * sigma
    hidden = (active * upper).astype(jnp.bfloat16)
    d_up = (hidden_grad * active).astype(jnp.bfloat16)
    d_gate = (hidden_grad * upper * sigma * (1.0 + gate * (1.0 - sigma))).astype(jnp.bfloat16)
    factor = float(inputs.shape[0] * groups) ** (-0.5)
    owned = width // groups
    hunits = w_gate.shape[1]
    gate_local = jnp.einsum("td,tf->df", inputs, d_gate, preferred_element_type=single) * factor
    gate_parts = lax.all_to_all(
        gate_local.reshape(owned, groups, hunits).astype(jnp.bfloat16),
        "rep",
        split_axis=1,
        concat_axis=1,
        tiled=True,
    ).astype(jnp.float32)
    grad_gate = jnp.sum(gate_parts, axis=1, keepdims=True)
    up_local = jnp.einsum("td,tf->df", inputs, d_up, preferred_element_type=single) * factor
    up_parts = lax.all_to_all(
        up_local.reshape(owned, groups, hunits).astype(jnp.bfloat16),
        "rep",
        split_axis=1,
        concat_axis=1,
        tiled=True,
    ).astype(jnp.float32)
    grad_up = jnp.sum(up_parts, axis=1, keepdims=True)
    down_local = jnp.einsum("tf,td->fd", hidden, own_cot, preferred_element_type=single) * factor
    down_parts = lax.all_to_all(
        down_local.reshape(hunits, owned, groups).astype(jnp.bfloat16),
        "rep",
        split_axis=2,
        concat_axis=2,
        tiled=True,
    ).astype(jnp.float32)
    grad_down = jnp.sum(down_parts, axis=2, keepdims=True)
    input_term = jnp.einsum("tf,df->td", d_gate, w_gate, preferred_element_type=single)
    input_term = input_term + jnp.einsum("tf,df->td", d_up, w_up, preferred_element_type=single)
    grad_input = lax.psum(input_term.astype(jnp.bfloat16), "tp")
    gate_norms, up_norms = lax.psum(
        (jnp.sum(grad_gate * grad_gate, axis=2), jnp.sum(grad_up * grad_up, axis=2)), "tp"
    )
    down_norms = lax.psum(jnp.sum(grad_down * grad_down, axis=(1, 2)), ("rep", "fs"))
    return (grad_input, grad_gate, grad_up, grad_down, gate_norms, up_norms, down_norms)


def solution(mesh):
    placed = (
        P("rep", "fs"),
        P("rep", "tp"),
        P("rep", "tp"),
        P("rep", None),
        P("fs", "tp"),
        P("fs", "tp"),
        P("tp", "fs"),
    )
    return jax.shard_map(
        on_device,
        mesh=mesh,
        in_specs=placed,
        out_specs=(
            P("rep", "fs"),
            P("fs", "rep", "tp"),
            P("fs", "rep", "tp"),
            P("tp", "fs", "rep"),
            P("fs", "rep"),
            P("fs", "rep"),
            P("tp"),
        ),
        check_vma=False,
    )
```

profile of v0, /device:TPU:10, one launch (start us, length us, event | category | flops | bytes accessed | tf_op | source)
XLA Modules:
  0.0 280.4 jit_solution(15499769138592350855)
XLA Ops:
  7.2 0.0 copy-start
  7.2 6.9 %multiply_convert_fusion = bf16[1408,1024]{0,1:T(8,128)(2,1)} fusion(bf16[640,1408]{1,0:T(8,128)(2,1)} %param.9, bf16[640,1408]{1,0:T(8,128)(2,1)} %param.8, bf16[640,2048]{1,0:T(8,128)(2,1)} %param.10, s32[]{:T(128)S(6)} %select_n.3), kind=kOutput, calls=%fused_computation.1 | convolution fusion | flops 1855586304 | bytes 7798788 | tf_op jit(solution)/shard_map/tf,td->fd/dot_general | solution.py:42
  14.1 5.7 %convert_element_type.74 = bf16[1408,256,4]{0,2,1:T(4,128)(2,1)} reshape(bf16[1408,1024]{0,1:T(8,128)(2,1)} %multiply_convert_fusion) | data formatting | bytes 5767168 | tf_op jit(solution)/shard_map/convert_element_type | solution.py:44
  19.8 3.8 %copy.16 = bf16[1408,256,4]{0,1,2:T(8,128)(2,1)} copy(bf16[1408,256,4]{0,2,1:T(4,128)(2,1)} %convert_element_type.74) | data formatting | bytes 5767168 | tf_op jit(solution)/shard_map/convert_element_type | solution.py:44
  23.6 5.3 %all-to-all-start.2 = ((bf16[1408,256,4]{0,1,2:T(8,128)(2,1)}), bf16[1408,256,4]{0,1,2:T(8,128)(2,1)}, u32[]{:S(2)}, u32[]{:S(2)}) async-start(bf16[1408,256,4]{0,1,2:T(8,128)(2,1)} %copy.16), calls=%async_computation.2 | async-start | bytes 5767168 | tf_op jit(solution)/shard_map/all_to_all | solution.py:43
  28.9 0.0 all-reduce.4.cloned.1.call-start
  28.9 0.0 copy-done
  28.9 4.8 %convolution_convert_fusion = bf16[640,1408]{1,0:T(8,128)(2,1)} fusion(bf16[1408,1024]{1,0:T(8,128)(2,1)S(1)} %copy-done, bf16[640,2048]{1,0:T(8,128)(2,1)} %param.10, s32[]{:T(128)S(6)} %select_n.3), kind=kOutput, calls=%fused_computation.23 | convolution fusion | flops 1846394880 | bytes 5996548 | tf_op jit(solution)/shard_map/td,fd->tf/dot_general | solution.py:12
  33.7 0.0 all-reduce.4.cloned.1.call-update
  33.7 57.6 %all-reduce.4.cloned.1.call-done = bf16[640,1408]{1,0:T(8,128)(2,1)} async-done(((bf16[640,1408]{1,0:T(8,128)(2,1)}), bf16[640,1408]{1,0:T(8,128)(2,1)}) %all-reduce.4.cloned.1.call-update) | async-done | bytes 1802256 | tf_op jit(solution)/shard_map/psum | solution.py:13
  91.3 6.7 %fusion.10 = bf16[1024,1408]{1,0:T(8,128)(2,1)} fusion(bf16[640,1024]{1,0:T(8,128)(2,1)} %param.7, bf16[640,1408]{1,0:T(8,128)(2,1)} %all-reduce.4.cloned.1.call-done, bf16[640,1408]{1,0:T(8,128)(2,1)} %param.8), kind=kOutput, calls=%fused_computation.22 | convolution fusion | flops 1855586304 | bytes 7798784 | tf_op jit(solution)/shard_map/td,tf->df/dot_general | solution.py:33
  98.0 4.6 %convert_element_type.70 = bf16[256,4,1408]{2,1,0:T(4,128)(2,1)S(1)} reshape(bf16[1024,1408]{1,0:T(8,128)(2,1)} %fusion.10) | data formatting | bytes 5767168 | tf_op jit(solution)/shard_map/convert_element_type | solution.py:35
  102.6 1.9 copy.15
  104.5 0.0 all-to-all-done.2
  104.5 5.1 %all-to-all-start.1 = ((bf16[256,4,1408]{2,0,1:T(8,128)(2,1)}), bf16[256,4,1408]{2,0,1:T(8,128)(2,1)S(1)}, u32[]{:S(2)}, u32[]{:S(2)}) async-start(bf16[256,4,1408]{2,0,1:T(8,128)(2,1)} %copy.15), calls=%async_computation.1 | async-start | bytes 5767168 | tf_op jit(solution)/shard_map/all_to_all | solution.py:34
  109.6 4.3 %fusion.3 = bf16[640,1408]{1,0:T(8,128)(2,1)S(1)} fusion(bf16[640,1408]{1,0:T(8,128)(2,1)} %param.9, bf16[640,1408]{1,0:T(8,128)(2,1)} %all-reduce.4.cloned.1.call-done, bf16[640,1408]{1,0:T(8,128)(2,1)} %param.8), kind=kLoop, calls=%fused_computation.15 | loop fusion | flops 11714560 | bytes 7208960 | tf_op jit(solution)/shard_map/convert_element_type | solution.py:20
  113.9 1.2 copy-done.7
  115.1 0.0 copy-done.9
  115.1 4.0 %fusion.9 = bf16[1024,1408]{1,0:T(8,128)(2,1)} fusion(bf16[640,1408]{1,0:T(8,128)(2,1)S(1)} %fusion.3, bf16[640,1024]{1,0:T(8,128)(2,1)S(1)} %copy-done.9), kind=kOutput, calls=%fused_computation.21 | convolution fusion | flops 1848377344 | bytes 5996544 | tf_op jit(solution)/shard_map/td,tf->df/dot_general | solution.py:24
  119.1 5.8 %convert_element_type.66 = bf16[256,4,1408]{2,1,0:T(4,128)(2,1)} reshape(bf16[1024,1408]{1,0:T(8,128)(2,1)} %fusion.9) | data formatting | bytes 5767168 | tf_op jit(solution)/shard_map/convert_element_type | solution.py:26
  124.9 3.8 %copy.14 = bf16[256,4,1408]{2,0,1:T(8,128)(2,1)} copy(bf16[256,4,1408]{2,1,0:T(4,128)(2,1)} %convert_element_type.66) | data formatting | bytes 5767168 | tf_op jit(solution)/shard_map/convert_element_type | solution.py:26
  128.6 42.6 %all-to-all-done.1 = bf16[256,4,1408]{2,0,1:T(8,128)(2,1)S(1)} async-done(((bf16[256,4,1408]{2,0,1:T(8,128)(2,1)}), bf16[256,4,1408]{2,0,1:T(8,128)(2,1)S(1)}, u32[]{:S(2)}, u32[]{:S(2)}) %all-to-all-start.1) | async-done | bytes 2883616 | tf_op jit(solution)/shard_map/all_to_all | solution.py:34
  171.2 1.7 copy-done.4
  172.9 7.8 %all-to-all-start = ((bf16[256,4,1408]{2,0,1:T(8,128)(2,1)}), bf16[256,4,1408]{2,0,1:T(8,128)(2,1)}, u32[]{:S(2)}, u32[]{:S(2)}) async-start(bf16[256,4,1408]{2,0,1:T(8,128)(2,1)} %copy.14), calls=%async_computation | async-start | bytes 5767168 | tf_op jit(solution)/shard_map/all_to_all | solution.py:25
  180.7 0.0 all-reduce.6.cloned.1.call-start
  180.8 4.7 %fusion.19 = f32[640,1024]{1,0:T(8,128)S(1)} fusion(bf16[640,1408]{1,0:T(8,128)(2,1)} %copy-done.7, bf16[1024,1408]{1,0:T(8,128)(2,1)} %param.11), kind=kOutput, calls=%fused_computation.33 | convolution fusion | flops 1845493760 | bytes 7307264 | tf_op jit(solution)/shard_map/tf,df->td/dot_general | solution.py:51
  185.5 0.0 copy-done.5
  185.5 0.0 copy-done.6
  185.5 0.0 copy-done.8
  185.5 3.5 %add_convert_fusion = bf16[640,1024]{1,0:T(8,128)(2,1)} fusion(f32[640,1024]{1,0:T(8,128)S(1)} %fusion.19, bf16[1024,1408]{1,0:T(8,128)(2,1)S(1)} %copy-done.8, bf16[640,1408]{1,0:T(8,128)(2,1)S(1)} %copy-done.6, bf16[640,1408]{1,0:T(8,128)(2,1)S(1)} %copy-done.5), kind=kOutput, calls=%fused_computation.24 | convolution fusion | flops 1854013440 | bytes 10420224 | tf_op jit(solution)/shard_map/tf,df->td/dot_general | solution.py:52
  189.0 0.0 all-reduce.6.cloned.1.call-update
  189.0 2.4 convert_reduce_fusion
  191.4 2.8 copy.18
  194.2 0.1 multiply_reduce_fusion
  194.3 59.8 %psum.39 = f32[1408]{0:T(1024)} all-reduce(f32[1408]{0:T(1024)S(1)} %multiply_reduce_fusion), channel_id=1, replica_groups=mesh['rep'=4,'fs'=2,'tp'=4] {'rep','fs'}, use_global_device_ids=true, to_apply=%region_10.0 | all-reduce | flops 1408 | bytes 11264 | tf_op jit(solution)/shard_map/psum | solution.py:57
  254.1 2.4 convert_reduce_fusion.1
  256.5 0.0 copy-start.2
  256.5 1.1 copy-done.2
  257.6 2.1 broadcast_in_dim.10
  259.7 0.0 all-to-all-done
  259.7 2.5 convert_reduce_fusion.2
  262.2 0.0 copy-start.1
  262.2 2.1 broadcast_in_dim.9
  264.3 0.0 copy-done.3
  264.3 0.2 multiply_reduce_fusion.1
  264.5 0.2 multiply_reduce_fusion.2
  264.6 6.5 %all-reduce = (f32[256,1]{0,1:T(1,128)}, f32[256,1]{0,1:T(1,128)}) all-reduce(f32[256,1]{0,1:T(1,128)S(1)} %bitcast.18, f32[256,1]{0,1:T(1,128)S(1)} %bitcast.17), channel_id=1, replica_groups=mesh['rep'=4,'fs'=2,'tp'=4] {'tp'}, use_global_device_ids=true, to_apply=%region_6.0 | all-reduce | flops 512 | bytes 4096 | tf_op jit(solution)/shard_map/psum | solution.py:54
  271.1 2.5 copy.22
  (9 shorter events, 0.0 us)
Async XLA Ops:
  7.2 21.7 %copy-start = (bf16[1408,1024]{1,0:T(8,128)(2,1)S(1)}, bf16[1408,1024]{1,0:T(8,128)(2,1)}, u32[]{:S(2)}) copy-start(bf16[1408,1024]{1,0:T(8,128)(2,1)} %param.13) | copy-start | bytes 8650756
  23.6 80.9 %all-to-all-start.2 = ((bf16[1408,256,4]{0,1,2:T(8,128)(2,1)}), bf16[1408,256,4]{0,1,2:T(8,128)(2,1)}, u32[]{:S(2)}, u32[]{:S(2)}) async-start(bf16[1408,256,4]{0,1,2:T(8,128)(2,1)} %copy.16), calls=%async_computation.2 | async-start | bytes 5767168 | tf_op jit(solution)/shard_map/all_to_all | solution.py:43
  28.9 62.4 %all-reduce.4.cloned.1.call-start = ((), (), s32[]{:S(2)}) async-start(), calls=%async_computation.3 | async-start | bytes 3604480 | tf_op jit(solution)/shard_map/psum | solution.py:13
  104.5 66.7 %all-to-all-start.1 = ((bf16[256,4,1408]{2,0,1:T(8,128)(2,1)}), bf16[256,4,1408]{2,0,1:T(8,128)(2,1)S(1)}, u32[]{:S(2)}, u32[]{:S(2)}) async-start(bf16[256,4,1408]{2,0,1:T(8,128)(2,1)} %copy.15), calls=%async_computation.1 | async-start | bytes 5767168 | tf_op jit(solution)/shard_map/all_to_all | solution.py:34
  109.6 5.5 %copy-start.9 = (bf16[640,1024]{1,0:T(8,128)(2,1)S(1)}, bf16[640,1024]{1,0:T(8,128)(2,1)}, u32[]{:S(2)}) copy-start(bf16[640,1024]{1,0:T(8,128)(2,1)} %param.7) | copy-start | bytes 3932164
  113.9 1.2 copy-start.7
  171.2 1.7 copy-start.4
  172.9 86.8 %all-to-all-start = ((bf16[256,4,1408]{2,0,1:T(8,128)(2,1)}), bf16[256,4,1408]{2,0,1:T(8,128)(2,1)}, u32[]{:S(2)}, u32[]{:S(2)}) async-start(bf16[256,4,1408]{2,0,1:T(8,128)(2,1)} %copy.14), calls=%async_computation | async-start | bytes 5767168 | tf_op jit(solution)/shard_map/all_to_all | solution.py:25
  180.7 4.7 %copy-start.5 = (bf16[640,1408]{1,0:T(8,128)(2,1)S(1)}, bf16[640,1408]{1,0:T(8,128)(2,1)}, u32[]{:S(2)}) copy-start(bf16[640,1408]{1,0:T(8,128)(2,1)} %param.8) | copy-start | bytes 5406724
  180.7 90.4 %all-reduce.6.cloned.1.call-start = ((), (), s32[]{:S(2)}) async-start(), calls=%async_computation.4 | async-start | bytes 2621440 | tf_op jit(solution)/shard_map/psum | solution.py:53
  180.7 4.8 %copy-start.6 = (bf16[640,1408]{1,0:T(8,128)(2,1)S(1)}, bf16[640,1408]{1,0:T(8,128)(2,1)}, u32[]{:S(2)}) copy-start(bf16[640,1408]{1,0:T(8,128)(2,1)} %all-reduce.4.cloned.1.call-done) | copy-start | bytes 5406724
  180.7 4.8 %copy-start.8 = (bf16[1024,1408]{1,0:T(8,128)(2,1)S(1)}, bf16[1024,1408]{1,0:T(8,128)(2,1)}, u32[]{:S(2)}) copy-start(bf16[1024,1408]{1,0:T(8,128)(2,1)} %param.12) | copy-start | bytes 8650756
  256.5 1.1 copy-start.2
  259.7 4.6 %copy-start.3 = (f32[256,1408]{1,0:T(8,128)S(1)}, f32[256,1408]{1,0:T(8,128)}, u32[]{:S(2)}) copy-start(f32[256,1408]{1,0:T(8,128)} %copy-done.2) | copy-start | bytes 4325380
  262.2 11.4 %copy-start.1 = (bf16[1408,1024]{1,0:T(8,128)(2,1)S(1)}, bf16[1408,1024]{1,0:T(8,128)(2,1)}, u32[]{:S(2)}) copy-start(bf16[1408,1024]{1,0:T(8,128)(2,1)} %param.13) | copy-start | bytes 8650756
Sparse Core Ops, SparseCore 0:
  33.8 57.4 all-reduce.3
  189.1 38.1 all-reduce.5
where the time goes:
time: 281 us; the launch traced here: 280 us
  waiting for transfers between devices  100 us (36%)
  blocking collectives  66.3 us (24%)
  local copies, waits for them, and re-layouts  39 us (14%)
  matrix products  30.5 us (11%)
  starting transfers between devices  18.3 us (7%)
  between operations  14.1 us (5%)
  other arithmetic  12 us (4%)
    psum x1, blocking collectives, on_device(): lax.psum(jnp.sum(grad_down * grad_down, axis=(1, 2)), ('rep', 'fs'))  59.8 us
    psum x1, waiting for transfers between devices, on_device(): lax.psum(partial_grad.astype(jnp.bfloat16), 'fs').astype(jnp.float32)  57.6 us
    all_to_all x1, waiting for transfers between devices, on_device(): lax.all_to_all(up_local.reshape(owned, groups, hunits).astype(jnp.bfloat1...  42.6 us
    convert_element_type x2, local copies, waits for them, and re-layouts, on_device(): gate_local.reshape(owned, groups, hunits).astype(jnp.bfloat16)  9.54 us
    convert_element_type x2, local copies, waits for them, and re-layouts, on_device(): down_local.reshape(hunits, owned, groups).astype(jnp.bfloat16)  9.5 us
    unnamed x22, local copies, waits for them, and re-layouts  9.25 us
    all_to_all x1, starting transfers between devices, on_device(): lax.all_to_all(gate_local.reshape(owned, groups, hunits).astype(jnp.bfloa...  7.83 us
    dot_general x1, matrix products, on_device(): jnp.einsum('tf,td->fd', hidden, own_cot, preferred_element_type=single)  6.89 us
  transfers between devices with their start and end apart: 5, of which 2 were waited for; matrix products, arithmetic and copies ran while one was open for 21% of the time, Pallas kernels for 0%

commit v1 on v0

--- a/solution.py
+++ b/solution.py
@@ -1,7 +1,17 @@
+import functools
+
 import jax
 import jax.numpy as jnp
 from jax import lax
+from jax.experimental import pallas as pl
+from jax.experimental.pallas import tpu as pltpu
 from jax.sharding import PartitionSpec as P
+
+LANES = 128
+F32 = jnp.float32
+BF16 = jnp.bfloat16
+MESH = pl.DeviceIdType.MESH
+NT = (((1,), (1,)), ((), ()))
 
 
 def on_device(inputs, gate_pre, up_pre, cotangent, w_gate, w_up, w_down):
@@ -58,6 +68,387 @@
     return (grad_input, grad_gate, grad_up, grad_down, gate_norms, up_norms, down_norms)
 
 
+def line_kernel(
+    sizes, x_hbm, gate_hbm, up_hbm, cot_hbm, wg_hbm, wu_hbm, wd_hbm,
+    gi_ref, out_ref, gu_norm_ref, down_norm_ref,
+    x_ref, gate_ref, up_ref, cot_ref, wg_ref, wu_ref, wd_ref,
+    left, right, pg_own, pg_peer, ab, bb, gi_acc, gi_own, gi_peer,
+    gu_own, gu_peer, dn_own, dn_peer,
+    load_sem, y_send, y_recv, a_send, a_recv, b_send, b_recv, c_send, c_recv,
+    gi_send, gi_recv, gg_send, gg_recv, gn_send, gn_recv, dn_send, dn_recv,
+):
+    n_fs, n_tp, factor = sizes
+    tokens, width = x_ref.shape
+    hunits = gate_ref.shape[1]
+    blocks = hunits // LANES
+    items = 3 * blocks
+    owned = width // 4
+    share = tokens // n_tp
+    rep, fs, tp = lax.axis_index("rep"), lax.axis_index("fs"), lax.axis_index("tp")
+    side = rep // 2
+    mid, end = 1 + side, 3 * side
+    far_mid, far_end = 2 - side, 3 - 3 * side
+    at_end = rep == end
+    partner = mid + end - rep
+    fs_peer = 1 - fs
+
+    loads = [
+        pltpu.make_async_copy(cot_hbm.at[:, pl.ds(pl.multiple_of(fs * width, LANES), width)], cot_ref, load_sem.at[0]),
+        pltpu.make_async_copy(wd_hbm, wd_ref, load_sem.at[1]),
+        pltpu.make_async_copy(gate_hbm, gate_ref, load_sem.at[2]),
+        pltpu.make_async_copy(up_hbm, up_ref, load_sem.at[3]),
+        pltpu.make_async_copy(x_hbm, x_ref, load_sem.at[4]),
+        pltpu.make_async_copy(wg_hbm, wg_ref, load_sem.at[5]),
+        pltpu.make_async_copy(wu_hbm, wu_ref, load_sem.at[6]),
+    ]
+    for load in loads:
+        load.start()
+
+    group = [(r, f) for r in range(4) for f in range(n_fs) if r or f]
+
+    def in_group(step):
+        return (lax.rem(rep + step[0], 4), lax.rem(fs + step[1], n_fs), tp)
+
+    def in_tp(step):
+        return (rep, fs, lax.rem(tp + step, n_tp))
+
+    barrier = pltpu.get_barrier_semaphore()
+    greeted = [in_group(s) for s in group] + [in_tp(s) for s in range(1, n_tp)]
+    for other in greeted:
+        pl.semaphore_signal(barrier, inc=1, device_id=other, device_id_type=MESH)
+    pl.semaphore_wait(barrier, len(greeted))
+
+    def remote(src, dst, send, recv, other):
+        return pltpu.make_async_remote_copy(
+            src_ref=src, dst_ref=dst, send_sem=send, recv_sem=recv, device_id=other, device_id_type=MESH
+        )
+
+    def y_copy(j):
+        return remote(pg_own.at[j], pg_peer.at[j], y_send.at[j], y_recv.at[j], (rep, fs_peer, tp))
+
+    def a_copy(t):
+        return remote(ab.at[t], ab.at[t], a_send.at[t], a_recv.at[t], (partner, fs, tp))
+
+    def b_copy(t):
+        return remote(ab.at[t, pl.ds(owned, 2 * owned)], bb.at[t], b_send.at[t], b_recv.at[t], (far_mid, fs, tp))
+
+    def c_copy(t):
+        return remote(
+            bb.at[t, pl.ds(owned, owned)], bb.at[t, pl.ds(0, owned)], c_send.at[t], c_recv.at[t], (partner, fs, tp)
+        )
+
+    def lanes(j):
+        return pl.ds(pl.multiple_of(j * LANES, LANES), LANES)
+
+    def term(kind, owner, t):
+        rows = pl.ds(pl.multiple_of(owner * owned, owned), owned)
+        return jnp.dot(left[kind, rows, :], right[t], preferred_element_type=F32) * factor
+
+    def loop(first, last, body):
+        def step(i, carry):
+            body(i)
+            return carry
+        lax.fori_loop(first, last, step, 0)
+
+    loads[0].wait()
+    loads[1].wait()
+
+    def partial_of(j):
+        rows = pl.ds(pl.multiple_of(j * LANES, LANES), LANES)
+        pg_own[j] = lax.dot_general(cot_ref[...], wd_ref[rows, :], NT, preferred_element_type=F32).astype(BF16)
+        y_copy(j).start()
+
+    loop(0, blocks, partial_of)
+
+    def spread(kind, source):
+        for b in range(4):
+            place = lax.broadcasted_iota(jnp.int32, (owned, width), 0) * 4 + b
+            pick = (place == lax.broadcasted_iota(jnp.int32, (owned, width), 1)).astype(F32).astype(BF16)
+            left[kind, b * owned:(b + 1) * owned, :] = lax.dot_general(
+                pick, source[...], NT, preferred_element_type=F32
+            ).astype(BF16)
+
+    spread(0, cot_ref)
+    loads[2].wait()
+    loads[3].wait()
+
+    def send_first(kind, t):
+        for slot, owner in enumerate((mid, far_mid, far_end)):
+            ab[t, slot * owned:(slot + 1) * owned, :] = term(kind, owner, t).astype(BF16)
+        a_copy(t).start()
+
+    def hidden_of(j):
+        g = gate_ref[:, lanes(j)].astype(F32)
+        u = up_ref[:, lanes(j)].astype(F32)
+        right[j] = (g * (1.0 / (1.0 + jnp.exp(-g))) * u).astype(BF16)
+
+        @pl.when(at_end)
+        def _():
+            send_first(0, j)
+
+    loop(0, blocks, hidden_of)
+    loads[4].wait()
+    spread(1, x_ref)
+
+    def pass_on(kind, t):
+        a_copy(t).wait_recv()
+        for slot, owner in ((1, far_mid), (2, far_end)):
+            rows = slice(slot * owned, (slot + 1) * owned)
+            ab[t, rows, :] = (ab[t, rows, :].astype(F32) + term(kind, owner, t)).astype(BF16)
+        b_copy(t).start()
+
+    def settle(kind, t):
+        b_copy(t).wait_recv()
+        bb[t, owned:, :] = (bb[t, owned:, :].astype(F32) + term(kind, end, t)).astype(BF16)
+        c_copy(t).start()
+        both = ab[t, :owned, :].astype(F32) + bb[t, :owned, :].astype(F32)
+        out_ref[t] = both + term(kind, mid, t)
+
+    def last_hop(kind, t):
+        c_copy(t).wait_recv()
+        out_ref[t] = bb[t, :owned, :].astype(F32) + term(kind, end, t)
+
+    lag = 2
+
+    def line(kind, first, last):
+        for t in range(first, first + lag):
+            pass_on(kind, t)
+
+        def step(t):
+            pass_on(kind, t)
+            settle(kind, t - lag)
+
+        loop(first + lag, last, step)
+
+    @pl.when(jnp.logical_not(at_end))
+    def _():
+        line(0, 0, blocks)
+
+    def grads_of(j):
+        y_copy(j).wait_recv()
+        g = gate_ref[:, lanes(j)].astype(F32)
+        u = up_ref[:, lanes(j)].astype(F32)
+        total = pg_own[j].astype(F32) + pg_peer[j].astype(F32)
+        s = 1.0 / (1.0 + jnp.exp(-g))
+        t = blocks + 2 * j
+        right[t] = (total * u * s * (1.0 + g * (1.0 - s))).astype(BF16)
+        right[t + 1] = (total * (g * s)).astype(BF16)
+
+        @pl.when(at_end)
+        def _():
+            send_first(1, t)
+            send_first(1, t + 1)
+
+    loop(0, blocks, grads_of)
+
+    loads[5].wait()
+    loads[6].wait()
+    gi_acc[...] = jnp.zeros_like(gi_acc)
+
+    def gi_term(j):
+        t = blocks + 2 * j
+        gi_acc[...] += lax.dot_general(right[t], wg_ref[:, lanes(j)], NT, preferred_element_type=F32) + lax.dot_general(
+            right[t + 1], wu_ref[:, lanes(j)], NT, preferred_element_type=F32
+        )
+
+    loop(0, blocks, gi_term)
+    gi_own[...] = gi_acc[...].astype(BF16)
+
+    def tokens_of(owner):
+        return pl.ds(pl.multiple_of(owner * share, share), share)
+
+    def gi_copy(step):
+        other = lax.rem(tp + step, n_tp)
+        return remote(
+            gi_own.at[tokens_of(other)], gi_peer.at[step - 1], gi_send.at[step - 1], gi_recv.at[step - 1], in_tp(step)
+        )
+
+    def gg_copy(step):
+        return remote(
+            gi_ref.at[tokens_of(tp)], gi_ref.at[tokens_of(tp)], gg_send.at[step - 1], gg_recv.at[step - 1], in_tp(step)
+        )
+
+    for step in range(1, n_tp):
+        gi_copy(step).start()
+
+    half = blocks + 2 * (blocks // 2)
+
+    @pl.when(at_end)
+    def _():
+        loop(0, blocks, functools.partial(last_hop, 0))
+
+    @pl.when(jnp.logical_not(at_end))
+    def _():
+        for t in range(blocks - lag, blocks):
+            settle(0, t)
+        line(1, blocks, half)
+
+    dn_own[...] = jnp.zeros_like(dn_own)
+    for j in range(blocks):
+        piece = out_ref[j]
+        dn_own[0:1, j * LANES:(j + 1) * LANES] = jnp.sum(piece * piece, axis=0, keepdims=True)
+
+    def dn_copy(k):
+        return remote(dn_own, dn_peer.at[k], dn_send.at[k], dn_recv.at[k], in_group(group[k]))
+
+    for k in range(len(group)):
+        dn_copy(k).start()
+
+    for step in range(1, n_tp):
+        gi_copy(step).wait_recv()
+    whole = gi_own[tokens_of(tp), :].astype(F32)
+    for step in range(1, n_tp):
+        whole += gi_peer[step - 1].astype(F32)
+    gi_ref[tokens_of(tp), :] = whole.astype(BF16)
+    for step in range(1, n_tp):
+        gg_copy(step).start()
+
+    @pl.when(at_end)
+    def _():
+        loop(blocks, items, functools.partial(last_hop, 1))
+
+    @pl.when(jnp.logical_not(at_end))
+    def _():
+        def step(t):
+            pass_on(1, t)
+            settle(1, t - lag)
+
+        loop(half, items, step)
+        for t in range(items - lag, items):
+            settle(1, t)
+
+    gu_own[...] = jnp.zeros_like(gu_own)
+    for kind in range(2):
+        squares = jnp.zeros((owned, LANES), F32)
+        for j in range(blocks):
+            piece = out_ref[blocks + 2 * j + kind]
+            squares += piece * piece
+        gu_own[kind:kind + 1, :] = jnp.sum(squares.T, axis=0, keepdims=True)
+
+    def gn_copy(step):
+        return remote(gu_own, gu_peer.at[step - 1], gn_send.at[step - 1], gn_recv.at[step - 1], in_tp(step))
+
+    for step in range(1, n_tp):
+        gn_copy(step).start()
+
+    for k in range(len(group)):
+        dn_copy(k).wait_recv()
+    down = dn_own[...]
+    for k in range(len(group)):
+        down += dn_peer[k]
+    down_norm_ref[...] = down
+
+    for step in range(1, n_tp):
+        gn_copy(step).wait_recv()
+    gate_up = gu_own[...]
+    for step in range(1, n_tp):
+        gate_up += gu_peer[step - 1]
+    gu_norm_ref[...] = gate_up
+
+    for step in range(1, n_tp):
+        gg_copy(step).wait_recv()
+        gg_copy(step).wait_send()
+        gi_copy(step).wait_send()
+        gn_copy(step).wait_send()
+    for k in range(len(group)):
+        dn_copy(k).wait_send()
+    loop(0, blocks, lambda j: y_copy(j).wait_send())
+
+    @pl.when(at_end)
+    def _():
+        loop(0, items, lambda t: a_copy(t).wait_send())
+
+    @pl.when(jnp.logical_not(at_end))
+    def _():
+        def drain(t):
+            b_copy(t).wait_send()
+            c_copy(t).wait_send()
+
+        loop(0, items, drain)
+
+
+def on_line(inputs, gate_pre, up_pre, cotangent, w_gate, w_up, w_down):
+    n_fs, n_tp = lax.axis_size("fs"), lax.axis_size("tp")
+    tokens, width = inputs.shape
+    hunits = w_gate.shape[1]
+    blocks = hunits // LANES
+    items = 3 * blocks
+    owned = width // 4
+    share = tokens // n_tp
+    n_group = 4 * n_fs - 1
+    dma = pltpu.SemaphoreType.DMA
+    vmem = pltpu.VMEM
+    sizes = (n_fs, n_tp, float(tokens * 4) ** (-0.5))
+    grad_input, parts, gate_up, down = pl.pallas_call(
+        functools.partial(line_kernel, sizes),
+        out_shape=(
+            jax.ShapeDtypeStruct((tokens, width), BF16),
+            jax.ShapeDtypeStruct((items, owned, LANES), F32),
+            jax.ShapeDtypeStruct((8, owned), F32),
+            jax.ShapeDtypeStruct((8, hunits), F32),
+        ),
+        in_specs=[pl.BlockSpec(memory_space=pl.ANY)] * 7,
+        out_specs=(pl.BlockSpec(memory_space=vmem),) * 4,
+        scratch_shapes=[
+            vmem((tokens, width), BF16),
+            vmem((tokens, hunits), BF16),
+            vmem((tokens, hunits), BF16),
+            vmem((tokens, width), BF16),
+            vmem((width, hunits), BF16),
+            vmem((width, hunits), BF16),
+            vmem((hunits, width), BF16),
+            vmem((2, width, tokens), BF16),
+            vmem((items, tokens, LANES), BF16),
+            vmem((blocks, tokens, LANES), BF16),
+            vmem((blocks, tokens, LANES), BF16),
+            vmem((items, 3 * owned, LANES), BF16),
+            vmem((items, 2 * owned, LANES), BF16),
+            vmem((tokens, width), F32),
+            vmem((tokens, width), BF16),
+            vmem((n_tp - 1, share, width), BF16),
+            vmem((8, owned), F32),
+            vmem((n_tp - 1, 8, owned), F32),
+            vmem((8, hunits), F32),
+            vmem((n_group, 8, hunits), F32),
+            dma((7,)),
+            dma((blocks,)), dma((blocks,)),
+            dma((items,)), dma((items,)),
+            dma((items,)), dma((items,)),
+            dma((items,)), dma((items,)),
+            dma((n_tp - 1,)), dma((n_tp - 1,)),
+            dma((n_tp - 1,)), dma((n_tp - 1,)),
+            dma((n_tp - 1,)), dma((n_tp - 1,)),
+            dma((n_group,)), dma((n_group,)),
+        ],
+        compiler_params=pltpu.CompilerParams(
+            collective_id=0, has_side_effects=True, vmem_limit_bytes=67043328
+        ),
+    )(inputs, gate_pre, up_pre, cotangent, w_gate, w_up, w_down)
+    grad_down = parts[:blocks].transpose(0, 2, 1).reshape(hunits, owned, 1)
+    pairs = parts[blocks:].reshape(blocks, 2, owned, LANES)
+    grad_gate = pairs[:, 0].transpose(1, 0, 2).reshape(owned, 1, hunits)
+    grad_up = pairs[:, 1].transpose(1, 0, 2).reshape(owned, 1, hunits)
+    return (
+        grad_input,
+        grad_gate,
+        grad_up,
+        grad_down,
+        gate_up[0].reshape(owned, 1),
+        gate_up[1].reshape(owned, 1),
+        down[0],
+    )
+
+
+def fits_line(mesh, inputs, w_gate):
+    n_rep, n_fs, n_tp = (mesh.shape[axis] for axis in ("rep", "fs", "tp"))
+    tokens, width = inputs.shape[0] // n_rep, inputs.shape[1] // n_fs
+    return (
+        n_rep == 4 and n_fs == 2 and n_tp > 1
+        and tokens % (16 * n_tp) == 0 and tokens % LANES == 0
+        and width % (4 * LANES) == 0 and (w_gate.shape[1] // n_tp) % LANES == 0
+    )
+
+
 def solution(mesh):
     placed = (
         P("rep", "fs"),
@@ -68,18 +459,19 @@
         P("fs", "tp"),
         P("tp", "fs"),
     )
-    return jax.shard_map(
-        on_device,
-        mesh=mesh,
-        in_specs=placed,
-        out_specs=(
-            P("rep", "fs"),
-            P("fs", "rep", "tp"),
-            P("fs", "rep", "tp"),
-            P("tp", "fs", "rep"),
-            P("fs", "rep"),
-            P("fs", "rep"),
-            P("tp"),
-        ),
-        check_vma=False,
+    out_placed = (
+        P("rep", "fs"),
+        P("fs", "rep", "tp"),
+        P("fs", "rep", "tp"),
+        P("tp", "fs", "rep"),
+        P("fs", "rep"),
+        P("fs", "rep"),
+        P("tp"),
     )
+
+    def whole(inputs, gate_pre, up_pre, cotangent, w_gate, w_up, w_down):
+        body = on_line if fits_line(mesh, inputs, w_gate) else on_device
+        mapped = jax.shard_map(body, mesh=mesh, in_specs=placed, out_specs=out_placed, check_vma=False)
+        return mapped(inputs, gate_pre, up_pre, cotangent, w_gate, w_up, w_down)
+
+    return whole

time: 281 us -> 202 us (0.72)
  the two profiles are of different devices: /device:TPU:10 before, /device:TPU:0 now
where the time goes in v1:
time: 202 us; the launch traced here: 201 us
  Pallas kernels  174 us (86%)
  local copies, waits for them, and re-layouts  26.5 us (13%)
    pallas_call x1, Pallas kernels, on_line(): pl.pallas_call(functools.partial(line_kernel, sizes), out_shape=(jax.Shap...  174 us
    unnamed x10, local copies, waits for them, and re-layouts  14.5 us
    transpose x2, local copies, waits for them, and re-layouts, on_line(): grad_down = parts[:blocks].transpose(0, 2, 1).reshape(hunits, owned, 1)  5.47 us

profile of v1, /device:TPU:0, one launch (start us, length us, event | category | flops | bytes accessed | tf_op | source)
XLA Modules:
  0.0 201.2 jit_solution(8068237752223981228)
XLA Ops:
  0.6 174.0 %shard_map.126 = (bf16[640,1024]{1,0:T(8,128)(2,1)}, f32[33,256,128]{2,1,0:T(8,128)}, f32[8,256]{1,0:T(8,128)}, f32[8,1408]{1,0:T(8,128)}) custom-call(bf16[640,1024]{1,0:T(8,128)(2,1)} %x_hbm.1, bf16[640,1408]{1,0:T(8,128)(2,1)} %gate_hbm.1, bf16[640,1408]{1,0:T(8,128)(2,1)} %up_hbm.1, bf16[640,2048]{1,0:T(8,128)(2,1)} %cot_hbm.1, ...), custom_call_target="tpu_custom_call" | custom-call | tf_op jit(solution)/shard_map/pallas_call | solution.py:382
  174.7 1.3 slice_bitcast_fusion.1
  176.0 1.4 slice_reduce_fusion
  177.4 2.6 %slice_bitcast_fusion = f32[11,128,256]{1,2,0:T(8,128)} fusion(f32[33,256,128]{2,1,0:T(8,128)} %get-tuple-element.12), kind=kLoop, calls=%fused_computation | loop fusion | bytes 2883584 | tf_op jit(solution)/shard_map/transpose | solution.py:427
  180.0 2.0 slice.21
  182.0 2.9 %copy.18 = f32[11,128,256]{2,1,0:T(8,128)} copy(f32[11,128,256]{1,2,0:T(8,128)} %slice_bitcast_fusion) | data formatting | bytes 2883584 | tf_op jit(solution)/shard_map/transpose | solution.py:427
  184.9 5.2 %copy.21 = f32[1408,256,1]{1,2,0:T(1,128)} copy(f32[1408,256,1]{1,0,2:T(8,128)} %bitcast.19) | data formatting | bytes 2883584
  190.1 1.8 fusion
  191.9 1.8 copy.23
  193.7 0.0 copy-start
  193.7 3.0 %copy.20 = f32[256,1,1408]{2,1,0:T(1,128)} copy(f32[256,1,1408]{0,2,1:T(8,128)S(1)} %bitcast.20) | data formatting | bytes 2883584
  196.7 0.0 copy-done
  196.7 0.4 copy.22
  197.1 0.0 copy-start.1
  197.2 3.0 %copy.19 = f32[256,1,1408]{2,1,0:T(1,128)} copy(f32[256,1,1408]{0,2,1:T(8,128)S(1)} %bitcast.21) | data formatting | bytes 2883584
  200.2 0.0 copy-done.1
  200.2 1.1 copy.25
Async XLA Ops:
  193.7 3.0 %copy-start = (f32[11,1,256,128]{3,2,1,0:T(8,128)S(1)}, f32[11,1,256,128]{3,2,1,0:T(8,128)}, u32[]{:S(2)}) copy-start(f32[11,1,256,128]{3,2,1,0:T(8,128)} %get-tuple-element.23) | copy-start | bytes 4325380
  197.1 3.0 %copy-start.1 = (bf16[640,1024]{1,0:T(8,128)(2,1)S(1)}, bf16[640,1024]{1,0:T(8,128)(2,1)}, u32[]{:S(2)}) copy-start(bf16[640,1024]{1,0:T(8,128)(2,1)} %get-tuple-element.33) | copy-start | bytes 3932164

commit v2 on v1

--- a/solution.py
+++ b/solution.py
@@ -70,11 +70,12 @@
 
 def line_kernel(
     sizes, x_hbm, gate_hbm, up_hbm, cot_hbm, wg_hbm, wu_hbm, wd_hbm,
-    gi_ref, out_ref, gu_norm_ref, down_norm_ref,
+    gi_ref, gate_out, up_out, down_out, gu_norm_ref, down_norm_ref,
     x_ref, gate_ref, up_ref, cot_ref, wg_ref, wu_ref, wd_ref,
-    left, right, pg_own, pg_peer, ab, bb, gi_acc, gi_own, gi_peer,
-    gu_own, gu_peer, dn_own, dn_peer,
+    left, left_far, right, right_far, pg_own, pg_peer, ab, sb, bb, gi_acc, gi_own, gi_peer,
+    squares, gu_own, gu_peer, dn_own, dn_peer,
     load_sem, y_send, y_recv, a_send, a_recv, b_send, b_recv, c_send, c_recv,
+    r_send, r_recv, f_send, f_recv, l_send, l_recv, m_send, m_recv,
     gi_send, gi_recv, gg_send, gg_recv, gn_send, gn_recv, dn_send, dn_recv,
 ):
     n_fs, n_tp, factor = sizes
@@ -129,20 +130,50 @@
     def a_copy(t):
         return remote(ab.at[t], ab.at[t], a_send.at[t], a_recv.at[t], (partner, fs, tp))
 
-    def b_copy(t):
-        return remote(ab.at[t, pl.ds(owned, 2 * owned)], bb.at[t], b_send.at[t], b_recv.at[t], (far_mid, fs, tp))
+    def b_copy(kind, t):
+        src = ab.at[t, pl.ds(owned, 2 * owned)] if kind == 0 else sb.at[t - blocks]
+        return remote(src, bb.at[t], b_send.at[t], b_recv.at[t], (far_mid, fs, tp))
 
     def c_copy(t):
         return remote(
             bb.at[t, pl.ds(owned, owned)], bb.at[t, pl.ds(0, owned)], c_send.at[t], c_recv.at[t], (partner, fs, tp)
         )
 
+    half = tokens // n_fs
+    own_half = pl.ds(pl.multiple_of(fs * half, 16), half)
+
+    def r_copy(q):
+        return remote(
+            right.at[blocks + q, own_half], right_far.at[q, own_half], r_send.at[q], r_recv.at[q], (partner, fs, tp)
+        )
+
+    def f_copy(q):
+        piece = right_far.at[q, own_half]
+        return remote(piece, piece, f_send.at[q], f_recv.at[q], (rep, fs_peer, tp))
+
+    piece_rows = 3 * owned // n_tp
+    own_piece = pl.ds(pl.multiple_of(tp * piece_rows, 16), piece_rows)
+
+    def l_copy():
+        return remote(left.at[1, own_piece], left_far.at[own_piece], l_send.at[0], l_recv.at[0], (partner, fs, tp))
+
+    def m_copy(step):
+        piece = left_far.at[own_piece]
+        return remote(piece, piece, m_send.at[step - 1], m_recv.at[step - 1], in_tp(step))
+
     def lanes(j):
         return pl.ds(pl.multiple_of(j * LANES, LANES), LANES)
 
-    def term(kind, owner, t):
-        rows = pl.ds(pl.multiple_of(owner * owned, owned), owned)
-        return jnp.dot(left[kind, rows, :], right[t], preferred_element_type=F32) * factor
+    def rows_of(slot):
+        return slice(slot * owned, (slot + 1) * owned)
+
+    def term(kind, slot, t):
+        return jnp.dot(left[kind, rows_of(slot), :], right[t], preferred_element_type=F32) * factor
+
+    def long_term(slot, t):
+        own = jnp.dot(left[1, rows_of(slot), :], right[t], preferred_element_type=F32)
+        far = jnp.dot(left_far[rows_of(slot), :], right_far[t - blocks], preferred_element_type=F32)
+        return (own + far) * factor
 
     def loop(first, last, body):
         def step(i, carry):
@@ -150,31 +181,40 @@
             return carry
         lax.fori_loop(first, last, step, 0)
 
+    lead = min(3, blocks - 1)
+    ahead = min(5, blocks)
+
     loads[0].wait()
     loads[1].wait()
 
     def partial_of(j):
         rows = pl.ds(pl.multiple_of(j * LANES, LANES), LANES)
         pg_own[j] = lax.dot_general(cot_ref[...], wd_ref[rows, :], NT, preferred_element_type=F32).astype(BF16)
-        y_copy(j).start()
+
+        @pl.when(jnp.logical_or(at_end, j < ahead))
+        def _():
+            y_copy(j).start()
 
     loop(0, blocks, partial_of)
 
     def spread(kind, source):
-        for b in range(4):
-            place = lax.broadcasted_iota(jnp.int32, (owned, width), 0) * 4 + b
+        for slot, owner in enumerate((mid, far_mid, far_end, end)):
+            place = lax.broadcasted_iota(jnp.int32, (owned, width), 0) * 4 + owner
             pick = (place == lax.broadcasted_iota(jnp.int32, (owned, width), 1)).astype(F32).astype(BF16)
-            left[kind, b * owned:(b + 1) * owned, :] = lax.dot_general(
+            left[kind, rows_of(slot), :] = lax.dot_general(
                 pick, source[...], NT, preferred_element_type=F32
             ).astype(BF16)
 
     spread(0, cot_ref)
     loads[2].wait()
     loads[3].wait()
-
-    def send_first(kind, t):
-        for slot, owner in enumerate((mid, far_mid, far_end)):
-            ab[t, slot * owned:(slot + 1) * owned, :] = term(kind, owner, t).astype(BF16)
+    squares[...] = jnp.zeros_like(squares)
+    dn_own[...] = jnp.zeros_like(dn_own)
+    gu_own[...] = jnp.zeros_like(gu_own)
+
+    def send_down(t):
+        for slot in range(3):
+            ab[t, rows_of(slot), :] = term(0, slot, t).astype(BF16)
         a_copy(t).start()
 
     def hidden_of(j):
@@ -182,47 +222,23 @@
         u = up_ref[:, lanes(j)].astype(F32)
         right[j] = (g * (1.0 / (1.0 + jnp.exp(-g))) * u).astype(BF16)
 
+    def hidden_first(j):
+        hidden_of(j)
+
         @pl.when(at_end)
         def _():
-            send_first(0, j)
-
-    loop(0, blocks, hidden_of)
+            send_down(j)
+
+    loop(0, 1, hidden_first)
     loads[4].wait()
     spread(1, x_ref)
 
-    def pass_on(kind, t):
-        a_copy(t).wait_recv()
-        for slot, owner in ((1, far_mid), (2, far_end)):
-            rows = slice(slot * owned, (slot + 1) * owned)
-            ab[t, rows, :] = (ab[t, rows, :].astype(F32) + term(kind, owner, t)).astype(BF16)
-        b_copy(t).start()
-
-    def settle(kind, t):
-        b_copy(t).wait_recv()
-        bb[t, owned:, :] = (bb[t, owned:, :].astype(F32) + term(kind, end, t)).astype(BF16)
-        c_copy(t).start()
-        both = ab[t, :owned, :].astype(F32) + bb[t, :owned, :].astype(F32)
-        out_ref[t] = both + term(kind, mid, t)
-
-    def last_hop(kind, t):
-        c_copy(t).wait_recv()
-        out_ref[t] = bb[t, :owned, :].astype(F32) + term(kind, end, t)
-
-    lag = 2
-
-    def line(kind, first, last):
-        for t in range(first, first + lag):
-            pass_on(kind, t)
-
-        def step(t):
-            pass_on(kind, t)
-            settle(kind, t - lag)
-
-        loop(first + lag, last, step)
-
-    @pl.when(jnp.logical_not(at_end))
-    def _():
-        line(0, 0, blocks)
+    @pl.when(at_end)
+    def _():
+        l_copy().start()
+
+    loop(1, lead, hidden_first)
+    loop(lead, blocks, hidden_of)
 
     def grads_of(j):
         y_copy(j).wait_recv()
@@ -234,12 +250,102 @@
         right[t] = (total * u * s * (1.0 + g * (1.0 - s))).astype(BF16)
         right[t + 1] = (total * (g * s)).astype(BF16)
 
-        @pl.when(at_end)
-        def _():
-            send_first(1, t)
-            send_first(1, t + 1)
-
-    loop(0, blocks, grads_of)
+    def finish(kind, j, piece):
+        if kind == 0:
+            dn_own[0:1, lanes(j)] = jnp.sum(piece * piece, axis=0, keepdims=True)
+            down_out[pl.ds(pl.multiple_of(j * LANES, LANES), LANES), 0, :] = piece.T
+        else:
+            squares[kind - 1] += piece * piece
+            (gate_out if kind == 1 else up_out)[:, 0, lanes(j)] = piece
+
+    def item(kind, j):
+        return j if kind == 0 else blocks + 2 * j + kind - 1
+
+    def down_on(t):
+        a_copy(t).wait_recv()
+        for slot in (1, 2):
+            ab[t, rows_of(slot), :] = (ab[t, rows_of(slot), :].astype(F32) + term(0, slot, t)).astype(BF16)
+        b_copy(0, t).start()
+
+    def forward(j):
+        for q in (2 * j, 2 * j + 1):
+            r_copy(q).wait_recv()
+            f_copy(q).start()
+
+    def pair_on(j):
+        for kind in (1, 2):
+            t = item(kind, j)
+            f_copy(t - blocks).wait_recv()
+            for slot in (1, 2):
+                sb[t - blocks, rows_of(slot - 1), :] = long_term(slot, t).astype(BF16)
+            b_copy(kind, t).start()
+
+    def settle(kind, j):
+        t = item(kind, j)
+        b_copy(kind, t).wait_recv()
+        bb[t, owned:, :] = (bb[t, owned:, :].astype(F32) + term(min(kind, 1), 3, t)).astype(BF16)
+        c_copy(t).start()
+        if kind == 0:
+            own = ab[t, :owned, :].astype(F32) + term(0, 0, t)
+        else:
+            own = long_term(0, t)
+        finish(kind, j, own + bb[t, :owned, :].astype(F32))
+
+    def last_hop(kind, j):
+        t = item(kind, j)
+        c_copy(t).wait_recv()
+        finish(kind, j, bb[t, :owned, :].astype(F32) + term(min(kind, 1), 3, t))
+
+    def through(action, j, with_down=True):
+        action(1, j)
+        action(2, j)
+        if with_down:
+            action(0, j + lead)
+
+    downs = blocks - lead
+    early = blocks - ahead
+
+    @pl.when(at_end)
+    def _():
+        def pair_out(j):
+            grads_of(j)
+            r_copy(2 * j).start()
+            r_copy(2 * j + 1).start()
+
+        def both_out(j):
+            pair_out(j)
+            send_down(j + lead)
+
+        loop(0, downs, both_out)
+        loop(downs, blocks, pair_out)
+
+    @pl.when(jnp.logical_not(at_end))
+    def _():
+        down_on(0)
+        l_copy().wait_recv()
+        for step in range(1, n_tp):
+            m_copy(step).start()
+        loop(1, lead, down_on)
+        forward(0)
+        for step in range(1, n_tp):
+            m_copy(step).wait_recv()
+        grads_of(0)
+        forward(1)
+        y_copy(ahead).start()
+        pair_on(0)
+        down_on(lead)
+        loop(0, lead, functools.partial(settle, 0))
+
+        def step(j):
+            grads_of(j)
+            forward(j + 1)
+            y_copy(ahead + j).start()
+            pair_on(j)
+            down_on(j + lead)
+            through(settle, j - 1)
+
+        loop(1, early, step)
+        loop(early, blocks, grads_of)
 
     loads[5].wait()
     loads[6].wait()
@@ -271,22 +377,23 @@
     for step in range(1, n_tp):
         gi_copy(step).start()
 
-    half = blocks + 2 * (blocks // 2)
-
     @pl.when(at_end)
     def _():
-        loop(0, blocks, functools.partial(last_hop, 0))
+        loop(0, lead, functools.partial(last_hop, 0))
+        loop(0, downs, functools.partial(through, last_hop))
 
     @pl.when(jnp.logical_not(at_end))
     def _():
-        for t in range(blocks - lag, blocks):
-            settle(0, t)
-        line(1, blocks, half)
-
-    dn_own[...] = jnp.zeros_like(dn_own)
-    for j in range(blocks):
-        piece = out_ref[j]
-        dn_own[0:1, j * LANES:(j + 1) * LANES] = jnp.sum(piece * piece, axis=0, keepdims=True)
+        def step(j):
+            forward(j + 1)
+            pair_on(j)
+            down_on(j + lead)
+            through(settle, j - 1)
+
+        loop(early, downs, step)
+        forward(downs + 1)
+        pair_on(downs)
+        through(settle, downs - 1)
 
     def dn_copy(k):
         return remote(dn_own, dn_peer.at[k], dn_send.at[k], dn_recv.at[k], in_group(group[k]))
@@ -305,25 +412,22 @@
 
     @pl.when(at_end)
     def _():
-        loop(blocks, items, functools.partial(last_hop, 1))
+        loop(downs, blocks, functools.partial(through, last_hop, with_down=False))
 
     @pl.when(jnp.logical_not(at_end))
     def _():
-        def step(t):
-            pass_on(1, t)
-            settle(1, t - lag)
-
-        loop(half, items, step)
-        for t in range(items - lag, items):
-            settle(1, t)
-
-    gu_own[...] = jnp.zeros_like(gu_own)
+        def step(j):
+            forward(j + 1)
+            pair_on(j)
+            through(settle, j - 1, with_down=False)
+
+        loop(downs + 1, blocks - 1, step)
+        pair_on(blocks - 1)
+        through(settle, blocks - 2, with_down=False)
+        through(settle, blocks - 1, with_down=False)
+
     for kind in range(2):
-        squares = jnp.zeros((owned, LANES), F32)
-        for j in range(blocks):
-            piece = out_ref[blocks + 2 * j + kind]
-            squares += piece * piece
-        gu_own[kind:kind + 1, :] = jnp.sum(squares.T, axis=0, keepdims=True)
+        gu_own[kind:kind + 1, :] = jnp.sum(squares[kind].T, axis=0, keepdims=True)
 
     def gn_copy(step):
         return remote(gu_own, gu_peer.at[step - 1], gn_send.at[step - 1], gn_recv.at[step - 1], in_tp(step))
@@ -356,15 +460,18 @@
 
     @pl.when(at_end)
     def _():
-        loop(0, items, lambda t: a_copy(t).wait_send())
+        l_copy().wait_send()
+        loop(0, blocks, lambda t: a_copy(t).wait_send())
+        loop(0, 2 * blocks, lambda q: r_copy(q).wait_send())
 
     @pl.when(jnp.logical_not(at_end))
     def _():
-        def drain(t):
-            b_copy(t).wait_send()
-            c_copy(t).wait_send()
-
-        loop(0, items, drain)
+        for step in range(1, n_tp):
+            m_copy(step).wait_send()
+        loop(0, blocks, lambda t: b_copy(0, t).wait_send())
+        loop(blocks, items, lambda t: b_copy(1, t).wait_send())
+        loop(0, items, lambda t: c_copy(t).wait_send())
+        loop(0, 2 * blocks, lambda q: f_copy(q).wait_send())
 
 
 def on_line(inputs, gate_pre, up_pre, cotangent, w_gate, w_up, w_down):
@@ -379,16 +486,18 @@
     dma = pltpu.SemaphoreType.DMA
     vmem = pltpu.VMEM
     sizes = (n_fs, n_tp, float(tokens * 4) ** (-0.5))
-    grad_input, parts, gate_up, down = pl.pallas_call(
+    grad_input, grad_gate, grad_up, grad_down, gate_up, down = pl.pallas_call(
         functools.partial(line_kernel, sizes),
         out_shape=(
             jax.ShapeDtypeStruct((tokens, width), BF16),
-            jax.ShapeDtypeStruct((items, owned, LANES), F32),
+            jax.ShapeDtypeStruct((owned, 1, hunits), F32),
+            jax.ShapeDtypeStruct((owned, 1, hunits), F32),
+            jax.ShapeDtypeStruct((hunits, 1, owned), F32),
             jax.ShapeDtypeStruct((8, owned), F32),
             jax.ShapeDtypeStruct((8, hunits), F32),
         ),
         in_specs=[pl.BlockSpec(memory_space=pl.ANY)] * 7,
-        out_specs=(pl.BlockSpec(memory_space=vmem),) * 4,
+        out_specs=(pl.BlockSpec(memory_space=vmem),) * 6,
         scratch_shapes=[
             vmem((tokens, width), BF16),
             vmem((tokens, hunits), BF16),
@@ -398,23 +507,31 @@
             vmem((width, hunits), BF16),
             vmem((hunits, width), BF16),
             vmem((2, width, tokens), BF16),
+            vmem((3 * owned, tokens), BF16),
             vmem((items, tokens, LANES), BF16),
+            vmem((2 * blocks, tokens, LANES), BF16),
             vmem((blocks, tokens, LANES), BF16),
             vmem((blocks, tokens, LANES), BF16),
-            vmem((items, 3 * owned, LANES), BF16),
+            vmem((blocks, 3 * owned, LANES), BF16),
+            vmem((2 * blocks, 2 * owned, LANES), BF16),
             vmem((items, 2 * owned, LANES), BF16),
             vmem((tokens, width), F32),
             vmem((tokens, width), BF16),
             vmem((n_tp - 1, share, width), BF16),
+            vmem((2, owned, LANES), F32),
             vmem((8, owned), F32),
             vmem((n_tp - 1, 8, owned), F32),
             vmem((8, hunits), F32),
             vmem((n_group, 8, hunits), F32),
             dma((7,)),
             dma((blocks,)), dma((blocks,)),
+            dma((blocks,)), dma((blocks,)),
             dma((items,)), dma((items,)),
             dma((items,)), dma((items,)),
-            dma((items,)), dma((items,)),
+            dma((2 * blocks,)), dma((2 * blocks,)),
+            dma((2 * blocks,)), dma((2 * blocks,)),
+            dma((1,)), dma((1,)),
+            dma((n_tp - 1,)), dma((n_tp - 1,)),
             dma((n_tp - 1,)), dma((n_tp - 1,)),
             dma((n_tp - 1,)), dma((n_tp - 1,)),
             dma((n_tp - 1,)), dma((n_tp - 1,)),
@@ -424,15 +541,11 @@
             collective_id=0, has_side_effects=True, vmem_limit_bytes=67043328
         ),
     )(inputs, gate_pre, up_pre, cotangent, w_gate, w_up, w_down)
-    grad_down = parts[:blocks].transpose(0, 2, 1).reshape(hunits, owned, 1)
-    pairs = parts[blocks:].reshape(blocks, 2, owned, LANES)
-    grad_gate = pairs[:, 0].transpose(1, 0, 2).reshape(owned, 1, hunits)
-    grad_up = pairs[:, 1].transpose(1, 0, 2).reshape(owned, 1, hunits)
     return (
         grad_input,
         grad_gate,
         grad_up,
-        grad_down,
+        grad_down.transpose(0, 2, 1),
         gate_up[0].reshape(owned, 1),
         gate_up[1].reshape(owned, 1),
         down[0],
@@ -443,7 +556,8 @@
     n_rep, n_fs, n_tp = (mesh.shape[axis] for axis in ("rep", "fs", "tp"))
     tokens, width = inputs.shape[0] // n_rep, inputs.shape[1] // n_fs
     return (
-        n_rep == 4 and n_fs == 2 and n_tp > 1
+        n_rep == 4 and n_fs == 2 and n_tp > 1 and w_gate.shape[1] // n_tp >= 10 * LANES
+        and (3 * width // 4) % (16 * n_tp) == 0
         and tokens % (16 * n_tp) == 0 and tokens % LANES == 0
         and width % (4 * LANES) == 0 and (w_gate.shape[1] // n_tp) % LANES == 0
     )

time: 202 us -> 167 us (0.83)
  Pallas kernels: 174 us -> 156 us
  local copies, waits for them, and re-layouts: 26.5 us -> 10.1 us
    pallas_call x1, Pallas kernels: 174 us -> 156 us  [on_line(): pl.pallas_call(functools.partial(line_kernel, sizes), out_shape=(jax.Shap...]
    unnamed x10, local copies, waits for them, and re-layouts: 14.5 us -> 7.33 us
    transpose x2 -> x0, local copies, waits for them, and re-layouts: 5.47 us -> none  [on_line(): grad_down = parts[:blocks].transpose(0, 2, 1).reshape(hunits, owned, 1)]
    slice x2 -> x0, local copies, waits for them, and re-layouts: 3.78 us -> none  [the longest x1 2.01 us: on_line(): pairs = parts[blocks:].reshape(blocks, 2, owned, LANES)]
where the time goes in v2:
time: 167 us
  Pallas kernels  156 us (93%)
  local copies, waits for them, and re-layouts  10.1 us (6%)
    pallas_call x1, Pallas kernels, on_line(): pl.pallas_call(functools.partial(line_kernel, sizes), out_shape=(jax.Shap...  156 us
    unnamed x10, local copies, waits for them, and re-layouts  7.33 us

profile of v2, /device:TPU:0, one launch (start us, length us, event | category | flops | bytes accessed | tf_op | source)
XLA Modules:
  0.0 166.7 jit_solution(7007364528948406817)
XLA Ops:
  0.6 155.9 %shard_map.126 = (bf16[640,1024]{1,0:T(8,128)(2,1)}, f32[256,1,1408]{2,1,0:T(1,128)}, f32[256,1,1408]{2,1,0:T(1,128)}, f32[1408,1,256]{2,1,0:T(1,128)}, f32[8,256]{1,0:T(8,128)}, /*index=5*/f32[8,1408]{1,0:T(8,128)}) custom-call(bf16[640,1024]{1,0:T(8,128)(2,1)} %x_hbm.1, bf16[640,1408]{1,0:T(8,128)(2,1)} %gate_hbm.1, bf16[640,1408]{1,0:T(8,128)(2,1)} %up_hbm.1, ...), custom_call_target="tpu_custom_call" | custom-call | tf_op jit(solution)/shard_map/pallas_call | solution.py:489
  156.5 0.0 copy-start.2
  156.5 1.4 slice_bitcast_fusion
  157.9 1.4 slice_reduce_fusion
  159.3 2.5 %copy.18 = bf16[640,1024]{1,0:T(8,128)(2,1)} copy(bf16[640,1024]{1,0:T(8,128)(2,1)} %get-tuple-element.28) | data formatting | bytes 2621440
  161.8 0.0 copy-done.2
  161.8 0.0 copy-start.1
  161.8 1.1 copy.19
  162.9 0.8 copy-done.1
  163.7 0.0 copy-start
  163.7 1.1 copy.20
  164.8 0.8 copy-done
  165.6 1.1 copy.21
Async XLA Ops:
  156.5 5.3 %copy-start.2 = (f32[256,1,1408]{2,1,0:T(1,128)S(1)}, f32[256,1,1408]{2,1,0:T(1,128)}, u32[]{:S(2)}) copy-start(f32[256,1,1408]{2,1,0:T(1,128)} %get-tuple-element.29) | copy-start | bytes 4325380
  161.8 1.9 %copy-start.1 = (f32[256,1,1408]{2,1,0:T(1,128)S(1)}, f32[256,1,1408]{2,1,0:T(1,128)}, u32[]{:S(2)}) copy-start(f32[256,1,1408]{2,1,0:T(1,128)} %get-tuple-element.30) | copy-start | bytes 4325380
  163.7 1.9 %copy-start = (f32[1408,1,256]{2,1,0:T(1,128)S(1)}, f32[1408,1,256]{2,1,0:T(1,128)}, u32[]{:S(2)}) copy-start(f32[1408,1,256]{2,1,0:T(1,128)} %get-tuple-element.16) | copy-start | bytes 4325380

commit v3 on v2

--- a/solution.py
+++ b/solution.py
@@ -102,8 +102,8 @@
         pltpu.make_async_copy(wg_hbm, wg_ref, load_sem.at[5]),
         pltpu.make_async_copy(wu_hbm, wu_ref, load_sem.at[6]),
     ]
-    for load in loads:
-        load.start()
+    for k in (0, 2, 3, 4, 1, 5, 6):
+        loads[k].start()
 
     group = [(r, f) for r in range(4) for f in range(n_fs) if r or f]
 
@@ -181,21 +181,8 @@
             return carry
         lax.fori_loop(first, last, step, 0)
 
-    lead = min(3, blocks - 1)
+    lead = min(2, blocks - 1)
     ahead = min(5, blocks)
-
-    loads[0].wait()
-    loads[1].wait()
-
-    def partial_of(j):
-        rows = pl.ds(pl.multiple_of(j * LANES, LANES), LANES)
-        pg_own[j] = lax.dot_general(cot_ref[...], wd_ref[rows, :], NT, preferred_element_type=F32).astype(BF16)
-
-        @pl.when(jnp.logical_or(at_end, j < ahead))
-        def _():
-            y_copy(j).start()
-
-    loop(0, blocks, partial_of)
 
     def spread(kind, source):
         for slot, owner in enumerate((mid, far_mid, far_end, end)):
@@ -205,6 +192,7 @@
                 pick, source[...], NT, preferred_element_type=F32
             ).astype(BF16)
 
+    loads[0].wait()
     spread(0, cot_ref)
     loads[2].wait()
     loads[3].wait()
@@ -238,6 +226,19 @@
         l_copy().start()
 
     loop(1, lead, hidden_first)
+
+    loads[1].wait()
+
+    def partial_of(j):
+        rows = pl.ds(pl.multiple_of(j * LANES, LANES), LANES)
+        pg_own[j] = lax.dot_general(cot_ref[...], wd_ref[rows, :], NT, preferred_element_type=F32).astype(BF16)
+
+        @pl.when(jnp.logical_or(at_end, j < ahead))
+        def _():
+            y_copy(j).start()
+
+    loop(0, blocks, partial_of)
+
     loop(lead, blocks, hidden_of)
 
     def grads_of(j):
@@ -302,6 +303,17 @@
         if with_down:
             action(0, j + lead)
 
+    def gi_term(j):
+        t = blocks + 2 * j
+        gi_acc[...] += lax.dot_general(right[t], wg_ref[:, lanes(j)], NT, preferred_element_type=F32) + lax.dot_general(
+            right[t + 1], wu_ref[:, lanes(j)], NT, preferred_element_type=F32
+        )
+
+    def grads_and_term(j):
+        grads_of(j)
+        gi_term(j)
+
+    gi_acc[...] = jnp.zeros_like(gi_acc)
     downs = blocks - lead
     early = blocks - ahead
 
@@ -318,9 +330,14 @@
 
         loop(0, downs, both_out)
         loop(downs, blocks, pair_out)
+        loads[5].wait()
+        loads[6].wait()
+        loop(0, blocks, gi_term)
 
     @pl.when(jnp.logical_not(at_end))
     def _():
+        loads[5].wait()
+        loads[6].wait()
         down_on(0)
         l_copy().wait_recv()
         for step in range(1, n_tp):
@@ -329,7 +346,7 @@
         forward(0)
         for step in range(1, n_tp):
             m_copy(step).wait_recv()
-        grads_of(0)
+        grads_and_term(0)
         forward(1)
         y_copy(ahead).start()
         pair_on(0)
@@ -342,22 +359,16 @@
             y_copy(ahead + j).start()
             pair_on(j)
             down_on(j + lead)
+            gi_term(j)
             through(settle, j - 1)
 
+            @pl.when(j > 1)
+            def _():
+                grads_and_term(ahead - 1 + j)
+
         loop(1, early, step)
-        loop(early, blocks, grads_of)
-
-    loads[5].wait()
-    loads[6].wait()
-    gi_acc[...] = jnp.zeros_like(gi_acc)
-
-    def gi_term(j):
-        t = blocks + 2 * j
-        gi_acc[...] += lax.dot_general(right[t], wg_ref[:, lanes(j)], NT, preferred_element_type=F32) + lax.dot_general(
-            right[t + 1], wu_ref[:, lanes(j)], NT, preferred_element_type=F32
-        )
-
-    loop(0, blocks, gi_term)
+        loop(ahead - 1 + early, blocks, grads_and_term)
+
     gi_own[...] = gi_acc[...].astype(BF16)
 
     def tokens_of(owner):

time: 167 us -> 153 us (0.916)
  Pallas kernels: 156 us -> 142 us
    pallas_call x1, Pallas kernels: 156 us -> 142 us  [on_line(): pl.pallas_call(functools.partial(line_kernel, sizes), out_shape=(jax.Shap...]
where the time goes in v3:
time: 153 us
  Pallas kernels  142 us (93%)
  local copies, waits for them, and re-layouts  10.1 us (7%)
    pallas_call x1, Pallas kernels, on_line(): pl.pallas_call(functools.partial(line_kernel, sizes), out_shape=(jax.Shap...  142 us
    unnamed x10, local copies, waits for them, and re-layouts  7.33 us

profile of v3, /device:TPU:0, one launch (start us, length us, event | category | flops | bytes accessed | tf_op | source)
XLA Modules:
  0.0 153.1 jit_solution(9924382792280325902)
XLA Ops:
  0.6 142.3 %shard_map.126 = (bf16[640,1024]{1,0:T(8,128)(2,1)}, f32[256,1,1408]{2,1,0:T(1,128)}, f32[256,1,1408]{2,1,0:T(1,128)}, f32[1408,1,256]{2,1,0:T(1,128)}, f32[8,256]{1,0:T(8,128)}, /*index=5*/f32[8,1408]{1,0:T(8,128)}) custom-call(bf16[640,1024]{1,0:T(8,128)(2,1)} %x_hbm.1, bf16[640,1408]{1,0:T(8,128)(2,1)} %gate_hbm.1, bf16[640,1408]{1,0:T(8,128)(2,1)} %up_hbm.1, ...), custom_call_target="tpu_custom_call" | custom-call | tf_op jit(solution)/shard_map/pallas_call | solution.py:500
  143.0 0.0 copy-start.2
  143.0 1.4 slice_bitcast_fusion
  144.4 1.4 slice_reduce_fusion
  145.8 2.5 %copy.18 = bf16[640,1024]{1,0:T(8,128)(2,1)} copy(bf16[640,1024]{1,0:T(8,128)(2,1)} %get-tuple-element.28) | data formatting | bytes 2621440
  148.3 0.0 copy-done.2
  148.3 0.0 copy-start.1
  148.3 1.1 copy.19
  149.4 0.8 copy-done.1
  150.2 0.0 copy-start
  150.2 1.1 copy.20
  151.3 0.8 copy-done
  152.0 1.1 copy.21
Async XLA Ops:
  143.0 5.3 %copy-start.2 = (f32[256,1,1408]{2,1,0:T(1,128)S(1)}, f32[256,1,1408]{2,1,0:T(1,128)}, u32[]{:S(2)}) copy-start(f32[256,1,1408]{2,1,0:T(1,128)} %get-tuple-element.29) | copy-start | bytes 4325380
  148.3 1.9 %copy-start.1 = (f32[256,1,1408]{2,1,0:T(1,128)S(1)}, f32[256,1,1408]{2,1,0:T(1,128)}, u32[]{:S(2)}) copy-start(f32[256,1,1408]{2,1,0:T(1,128)} %get-tuple-element.30) | copy-start | bytes 4325380
  150.2 1.9 %copy-start = (f32[1408,1,256]{2,1,0:T(1,128)S(1)}, f32[1408,1,256]{2,1,0:T(1,128)}, u32[]{:S(2)}) copy-start(f32[1408,1,256]{2,1,0:T(1,128)} %get-tuple-element.16) | copy-start | bytes 4325380
